TPU v7x, 32 devices: a whole 2x2x4 slice. The times are simulated.
32 devices in a mesh: grp: 2 (over y), sp: 4 (over z), tp: 4 (over x, core).
Axes of the slice: x: 2, y: 2, z: 4, core: 2. Of those that a mesh axis runs over, the one named last changes fastest.
Arguments:
- tokens_in: bfloat16 [2048, 2048], P(('grp', 'sp'), 'tp'), parts along dimension 0, may hold values from -6 to 6
- norm_gain: float32 [3, 2048], replicated, may hold values from 0.1 to 1.9
- w_pool_in: bfloat16 [3, 2048, 1024], P(None, 'sp', 'tp'), may hold values from -0.125 to 0.125
- w_gate: bfloat16 [3, 2048, 2048], P(None, 'sp', 'tp'), may hold values from -0.125 to 0.125
- w_back: bfloat16 [3, 1024, 2048], P(None, 'tp', 'sp'), may hold values from -0.25 to 0.25
Outputs:
- tokens_out: bfloat16 [2048, 2048], P(('grp', 'sp'), 'tp'), parts along dimension 0
There are 2 independent parts, one for each index of `grp`. A program takes and returns all parts, laid end to end along the dimension named above; an argument that names none is the same for every part. Nothing has to cross between parts.
All inputs are finite; a program needn't handle non-finite values.
Results may differ from a plain program's by a relative error of at most 0.017.
Values may be sent and summed in bfloat16 or wider, within the bound.
A program may use at most 64 MiB of HBM per device.

v0:
```python
import jax
import jax.numpy as jnp
from jax import lax
from jax.sharding import PartitionSpec as P

POOL_WIDTH = 1024
GROUPS = 4
GRID_W = 32
LAYERS = 3
pool_windows = (2, 4, 8, 16)
norm_eps = 1e-06


def padded_2(value, sides, width):
    for axis, dim in sides:
        peers, length = (lax.axis_size(axis), value.shape[dim])
        up = [(i, (i + 1) % peers) for i in range(peers - 1)]
        down = [(j, i) for i, j in up]
        last = lax.slice_in_dim(value, length - width, length, axis=dim)
        initial = lax.slice_in_dim(value, 0, width, axis=dim)
        before = lax.ppermute(last, axis, up)
        after = lax.ppermute(initial, axis, down)
        value = jnp.concatenate([before, value, after], axis=dim)
    return value


def window_means(padded, rows_here, first_row, total_rows, window):
    reach = max(pool_windows) // 2
    half_span = window // 2
    width_cols = padded.shape[1] - 2 * reach
    row_sums = padded[reach - half_span : reach - half_span + rows_here]
    for offset in range(1 - half_span, half_span):
        row_sums = row_sums + padded[reach + offset : reach + offset + rows_here]
    box_sums = row_sums[:, reach - half_span : reach - half_span + width_cols]
    for offset in range(1 - half_span, half_span):
        box_sums = box_sums + row_sums[:, reach + offset : reach + offset + width_cols]
    row_index = first_row + jnp.arange(rows_here, dtype=jnp.int32)
    col_index = jnp.arange(width_cols, dtype=jnp.int32)
    row_counts = jnp.minimum(row_index + half_span, total_rows) - jnp.maximum(
        row_index - half_span, 0
    )
    col_counts = jnp.minimum(col_index + half_span, width_cols) - jnp.maximum(
        col_index - half_span, 0
    )
    counts = (row_counts[:, None] * col_counts[None, :]).astype(jnp.float32)
    return box_sums / counts[:, :, None]


def on_device(tokens_in, norm_gain, w_pool_in, w_gate, w_back):
    reach = max(pool_windows) // 2
    sp_count = lax.axis_size("sp")
    tp_count = lax.axis_size("tp")
    tp_pos = lax.axis_index("tp")
    sp_pos = lax.axis_index("sp")
    tok_rows = tokens_in.shape[0]
    rows_here = tok_rows // GRID_W
    total_rows = rows_here * sp_count
    first_row = sp_pos * rows_here
    local_pool = w_pool_in.shape[2]
    group_width = POOL_WIDTH // GROUPS
    channel_group = (tp_pos * local_pool + jnp.arange(local_pool, dtype=jnp.int32)) // group_width
    state = tokens_in
    for layer_id in range(LAYERS):
        whole_rows = lax.all_gather(state, "tp", axis=1, tiled=True)
        wide = whole_rows.astype(jnp.float32)
        normed = (
            wide
            * lax.rsqrt(jnp.mean(wide * wide, axis=-1, keepdims=True) + norm_eps)
            * norm_gain[layer_id]
        ).astype(jnp.bfloat16)
        pool_acc = jnp.dot(
            normed,
            lax.all_gather(w_pool_in[layer_id], "sp", axis=0, tiled=True),
            preferred_element_type=jnp.float32,
        )
        gate_acc = jnp.dot(
            normed,
            lax.all_gather(w_gate[layer_id], "sp", axis=0, tiled=True),
            preferred_element_type=jnp.float32,
        )
        pool_in = pool_acc.astype(jnp.bfloat16)
        gate = jax.nn.sigmoid(gate_acc)
        cells = pool_in.reshape(rows_here, GRID_W, local_pool)
        rimmed = padded_2(cells, (("sp", 0),), reach)
        padded = jnp.pad(rimmed.astype(jnp.float32), ((0, 0), (reach, reach), (0, 0)))
        means = jnp.zeros((rows_here, GRID_W, local_pool), jnp.float32)
        for group_id in range(GROUPS):
            in_group = (channel_group == group_id)[None, None, :]
            means = jnp.where(
                in_group,
                window_means(padded, rows_here, first_row, total_rows, pool_windows[group_id]),
                means,
            )
        pooled = (
            (means - cells.astype(jnp.float32)).reshape(tok_rows, local_pool).astype(jnp.bfloat16)
        )
        full_pooled = lax.all_gather(pooled, "tp", axis=1, tiled=True)
        back_rows = lax.all_gather(w_back[layer_id], "sp", axis=1, tiled=True)
        back_cols = lax.all_to_all(back_rows, "tp", split_axis=1, concat_axis=0, tiled=True)
        partials = jnp.einsum(
            "tnb,nbd->ntd",
            full_pooled.reshape(tok_rows, tp_count, local_pool),
            back_cols.reshape(tp_count, local_pool, back_cols.shape[1]),
            preferred_element_type=jnp.float32,
        ).astype(jnp.bfloat16)
        branch = jnp.sum(partials.astype(jnp.float32), axis=0)
        state = (state.astype(jnp.float32) + gate * branch).astype(jnp.bfloat16)
    return state


def solution(mesh):
    return jax.shard_map(
        on_device,
        mesh=mesh,
        in_specs=(
            P(("grp", "sp"), "tp"),
            P(),
            P(None, "sp", "tp"),
            P(None, "sp", "tp"),
            P(None, "tp", "sp"),
        ),
        out_specs=P(("grp", "sp"), "tp"),
        check_vma=False,
    )
```

profile of v0, /device:TPU:0, one launch (start us, length us, event | category | flops | bytes accessed | tf_op | source)
XLA Modules:
  0.0 391.0 jit_solution(7945444731493379469)
XLA Ops:
  6.5 0.7 all-gather.22.cloned.1.call-update
  7.3 2.2 fusion.168
  9.6 0.8 fusion.167
  10.3 0.8 copy.33
  11.3 1.2 fusion.166
  12.9 0.6 fusion.169
  13.5 14.9 %all-gather.22.cloned.1.call-done = bf16[256,2048]{1,0:T(8,128)(2,1)} async-done(((bf16[256,512]{1,0:T(8,128)(2,1)}), bf16[256,2048]{1,0:T(8,128)(2,1)}) %all-gather.22.cloned.1.call-update) | async-done | bytes 1048592 | tf_op jit(solution)/shard_map/all_gather | solution.py:64
  28.3 1.5 fusion
  29.9 28.1 %all-gather.30.cloned.1.call-done = bf16[1,2048,256]{2,1,0:T(8,128)(2,1)} async-done(((bf16[1,512,256]{2,1,0:T(8,128)(2,1)}), bf16[1,2048,256]{2,1,0:T(8,128)(2,1)}) %all-gather.30.cloned.1.call-update) | async-done | bytes 1048592 | tf_op jit(solution)/shard_map/all_gather | solution.py:73
  57.9 2.0 convolution_convert_fusion.5
  60.0 3.4 collective-permute-start
  63.3 1.3 collective-permute-start.1
  64.7 23.0 %all-gather.32.cloned.1.call-done = bf16[1,256,2048]{1,2,0:T(8,128)(2,1)} async-done(((bf16[1,256,512]{1,2,0:T(8,128)(2,1)}), bf16[1,256,2048]{1,2,0:T(8,128)(2,1)}) %all-gather.32.cloned.1.call-update) | async-done | bytes 1048592 | tf_op jit(solution)/shard_map/all_gather | solution.py:98
  87.7 2.3 copy.20
  90.0 3.5 all-to-all-start
  94.1 0.8 fusion.151
  94.9 16.6 %all_gather.48 = bf16[256,1024]{1,0:T(8,128)(2,1)S(1)} all-gather(bf16[256,256]{1,0:T(8,128)(2,1)S(1)} %bitcast.112), channel_id=1, replica_groups=mesh['grp'=2,'sp'=4,'tp'=4] {'tp'}, dimensions={1}, use_global_device_ids=true | all-gather | bytes 655360 | tf_op jit(solution)/shard_map/all_gather | solution.py:97
  112.3 21.1 %all-gather.28.cloned.1.call-done = bf16[1,2048,512]{2,1,0:T(8,128)(2,1)} async-done(((bf16[1,512,512]{2,1,0:T(8,128)(2,1)}), bf16[1,2048,512]{2,1,0:T(8,128)(2,1)}) %all-gather.28.cloned.1.call-update) | async-done | bytes 2097168 | tf_op jit(solution)/shard_map/all_gather | solution.py:78
  133.4 3.2 fusion.75
  137.2 0.8 copy.34
  138.1 0.7 all-gather.34.cloned.1.call-update
  138.8 13.4 %all-gather.24.cloned.1.call-done = bf16[256,2048]{1,0:T(8,128)(2,1)} async-done(((bf16[256,512]{1,0:T(8,128)(2,1)}), bf16[256,2048]{1,0:T(8,128)(2,1)}) %all-gather.24.cloned.1.call-update) | async-done | bytes 1048592 | tf_op jit(solution)/shard_map/all_gather | solution.py:64
  152.2 1.5 fusion.3
  153.8 27.9 %all-gather.36.cloned.1.call-done = bf16[1,2048,256]{2,1,0:T(8,128)(2,1)} async-done(((bf16[1,512,256]{2,1,0:T(8,128)(2,1)}), bf16[1,2048,256]{2,1,0:T(8,128)(2,1)}) %all-gather.36.cloned.1.call-update) | async-done | bytes 1048592 | tf_op jit(solution)/shard_map/all_gather | solution.py:73
  181.7 2.0 convolution_convert_fusion.4
  183.7 3.4 collective-permute-start.2
  187.1 1.3 collective-permute-start.3
  188.4 23.1 %all-gather.38.cloned.1.call-done = bf16[1,256,2048]{1,2,0:T(8,128)(2,1)} async-done(((bf16[1,256,512]{1,2,0:T(8,128)(2,1)}), bf16[1,256,2048]{1,2,0:T(8,128)(2,1)}) %all-gather.38.cloned.1.call-update) | async-done | bytes 1048592 | tf_op jit(solution)/shard_map/all_gather | solution.py:98
  211.5 2.3 copy.24
  213.7 3.5 all-to-all-start.1
  218.4 0.8 fusion.152
  219.2 16.1 %all_gather.53 = bf16[256,1024]{1,0:T(8,128)(2,1)S(1)} all-gather(bf16[256,256]{1,0:T(8,128)(2,1)S(1)} %bitcast.113), channel_id=1, replica_groups=mesh['grp'=2,'sp'=4,'tp'=4] {'tp'}, dimensions={1}, use_global_device_ids=true | all-gather | bytes 655360 | tf_op jit(solution)/shard_map/all_gather | solution.py:97
  236.0 21.2 %all-gather.34.cloned.1.call-done = bf16[1,2048,512]{2,1,0:T(8,128)(2,1)} async-done(((bf16[1,512,512]{2,1,0:T(8,128)(2,1)}), bf16[1,2048,512]{2,1,0:T(8,128)(2,1)}) %all-gather.34.cloned.1.call-update) | async-done | bytes 2097168 | tf_op jit(solution)/shard_map/all_gather | solution.py:78
  257.3 3.1 fusion.72
  261.1 0.8 copy.35
  262.5 13.6 %all-gather.26.cloned.1.call-done = bf16[256,2048]{1,0:T(8,128)(2,1)} async-done(((bf16[256,512]{1,0:T(8,128)(2,1)}), bf16[256,2048]{1,0:T(8,128)(2,1)}) %all-gather.26.cloned.1.call-update) | async-done | bytes 1048592 | tf_op jit(solution)/shard_map/all_gather | solution.py:64
  276.1 1.5 fusion.6
  277.6 27.9 %all-gather.42.cloned.1.call-done = bf16[1,2048,256]{2,1,0:T(8,128)(2,1)} async-done(((bf16[1,512,256]{2,1,0:T(8,128)(2,1)}), bf16[1,2048,256]{2,1,0:T(8,128)(2,1)}) %all-gather.42.cloned.1.call-update) | async-done | bytes 1048592 | tf_op jit(solution)/shard_map/all_gather | solution.py:73
  305.5 2.0 convolution_convert_fusion.3
  307.6 3.4 collective-permute-start.4
  310.9 1.3 collective-permute-start.5
  312.2 23.1 %all-gather.44.cloned.1.call-done = bf16[1,256,2048]{1,2,0:T(8,128)(2,1)} async-done(((bf16[1,256,512]{1,2,0:T(8,128)(2,1)}), bf16[1,256,2048]{1,2,0:T(8,128)(2,1)}) %all-gather.44.cloned.1.call-update) | async-done | bytes 1048592 | tf_op jit(solution)/shard_map/all_gather | solution.py:98
  335.3 2.3 copy.28
  337.6 3.7 all-to-all-start.2
  342.3 0.8 fusion.153
  343.1 16.1 %all_gather.58 = bf16[256,1024]{1,0:T(8,128)(2,1)S(1)} all-gather(bf16[256,256]{1,0:T(8,128)(2,1)S(1)} %bitcast.111), channel_id=1, replica_groups=mesh['grp'=2,'sp'=4,'tp'=4] {'tp'}, dimensions={1}, use_global_device_ids=true | all-gather | bytes 655360 | tf_op jit(solution)/shard_map/all_gather | solution.py:97
  359.9 21.1 %all-gather.40.cloned.1.call-done = bf16[1,2048,512]{2,1,0:T(8,128)(2,1)} async-done(((bf16[1,512,512]{2,1,0:T(8,128)(2,1)}), bf16[1,2048,512]{2,1,0:T(8,128)(2,1)}) %all-gather.40.cloned.1.call-update) | async-done | bytes 2097168 | tf_op jit(solution)/shard_map/all_gather | solution.py:78
  381.0 3.1 fusion.69
  (113 shorter events, 7.0 us)
Async XLA Ops:
  6.5 3.0 copy-start.5
  6.5 21.8 %all-gather.22.cloned.1.call-start = ((), (), s32[]{:S(2)}) async-start(), calls=%async_computation.3 | async-start | bytes 1310720 | tf_op jit(solution)/shard_map/all_gather | solution.py:64
  7.3 4.0 %copy-start = (bf16[3,512,512]{2,1,0:T(8,128)(2,1)S(1)}, bf16[3,512,512]{2,1,0:T(8,128)(2,1)}, u32[]{:S(2)}) copy-start(bf16[3,512,512]{2,1,0:T(8,128)(2,1)} %param.8) | copy-start | bytes 4718596
  7.3 50.7 %all-gather.30.cloned.1.call-start = ((), (), s32[]{:S(2)}) async-start(), calls=%async_computation.7 | async-start | bytes 1310720 | tf_op jit(solution)/shard_map/all_gather | solution.py:73
  9.5 78.2 %all-gather.32.cloned.1.call-start = ((), (), s32[]{:S(2)}) async-start(), calls=%async_computation.8 | async-start | bytes 1310720 | tf_op jit(solution)/shard_map/all_gather | solution.py:98
  11.2 1.7 copy-start.6
  11.2 122.2 %all-gather.28.cloned.1.call-start = ((), (), s32[]{:S(2)}) async-start(), calls=%async_computation.6 | async-start | bytes 2621440 | tf_op jit(solution)/shard_map/all_gather | solution.py:78
  13.5 46.5 %copy-start.10 = (f32[1,2048]{1,0:T(1,128)}, f32[1,2048]{1,0:T(1,128)S(1)}, u32[]{:S(2)}) copy-start(f32[1,2048]{1,0:T(1,128)S(1)} %get-tuple-element.27) | copy-start | bytes 24580
  29.9 60.1 %copy-start.23 = (f32[256]{0:T(256)}, f32[256]{0:T(256)S(1)}, u32[]{:S(2)}) copy-start(f32[256]{0:T(256)S(1)} %add_rsqrt_fusion.2) | copy-start | bytes 3076
  60.0 33.6 %collective-permute-start = (bf16[8,32,256]{2,1,0:T(8,128)(2,1)S(1)}, bf16[8,32,256]{2,1,0:T(8,128)(2,1)S(1)}, u32[]{:S(2)}, u32[]{:S(2)}) collective-permute-start(bf16[8,32,256]{2,1,0:T(8,128)(2,1)S(1)} %bitcast.99), channel_id=1, source_target_pairs={{0,4},{4,8},{8,12},{1,5},{5,9},{9,13},{2,6},{6,10},{10,14},{3,7},{... | collective-permute-start | bytes 393224 | tf_op jit(solution)/shard_map/ppermute | solution.py:21
  63.3 30.2 %collective-permute-start.1 = (bf16[8,32,256]{2,1,0:T(8,128)(2,1)S(1)}, bf16[8,32,256]{2,1,0:T(8,128)(2,1)S(1)}, u32[]{:S(2)}, u32[]{:S(2)}) collective-permute-start(bf16[8,32,256]{2,1,0:T(8,128)(2,1)S(1)} %bitcast.100), channel_id=1, source_target_pairs={{4,0},{8,4},{12,8},{5,1},{9,5},{13,9},{6,2},{10,6},{14,10},{7,3},{... | collective-permute-start | bytes 393224 | tf_op jit(solution)/shard_map/ppermute | solution.py:22
  64.7 29.4 %copy-start.11 = (pred[256]{0:T(512)(128)(4,1)}, pred[256]{0:T(512)(128)(4,1)S(1)}, u32[]{:S(2)}) copy-start(pred[256]{0:T(512)(128)(4,1)S(1)} %get-tuple-element.33) | copy-start | bytes 772
  64.7 29.4 %copy-start.14 = (pred[256]{0:T(512)(128)(4,1)}, pred[256]{0:T(512)(128)(4,1)S(1)}, u32[]{:S(2)}) copy-start(pred[256]{0:T(512)(128)(4,1)S(1)} %get-tuple-element.34) | copy-start | bytes 772
  64.7 29.4 %copy-start.17 = (pred[256]{0:T(512)(128)(4,1)}, pred[256]{0:T(512)(128)(4,1)S(1)}, u32[]{:S(2)}) copy-start(pred[256]{0:T(512)(128)(4,1)S(1)} %get-tuple-element.35) | copy-start | bytes 772
  64.7 29.4 %copy-start.20 = (pred[256]{0:T(512)(128)(4,1)}, pred[256]{0:T(512)(128)(4,1)S(1)}, u32[]{:S(2)}) copy-start(pred[256]{0:T(512)(128)(4,1)S(1)} %get-tuple-element.36) | copy-start | bytes 772
  90.0 21.8 %all-to-all-start = ((bf16[256,4,512]{2,0,1:T(8,128)(2,1)}), bf16[256,4,512]{2,0,1:T(8,128)(2,1)S(1)}, u32[]{:S(2)}, u32[]{:S(2)}) async-start(bf16[256,4,512]{2,0,1:T(8,128)(2,1)} %copy.20), calls=%async_computation | async-start | bytes 2097152 | tf_op jit(solution)/shard_map/all_to_all | solution.py:99
  93.5 58.7 %all-gather.24.cloned.1.call-start = ((), (), s32[]{:S(2)}) async-start(), calls=%async_computation.4 | async-start | bytes 1310720 | tf_op jit(solution)/shard_map/all_gather | solution.py:64
  94.9 38.5 %copy-start.1 = (bf16[256,2048]{1,0:T(8,128)(2,1)S(1)}, bf16[256,2048]{1,0:T(8,128)(2,1)}, u32[]{:S(2)}) copy-start(bf16[256,2048]{1,0:T(8,128)(2,1)} %all-gather.22.cloned.1.call-done) | copy-start | bytes 3145732
  112.3 24.9 %copy-start.4 = (bf16[1,256,512]{2,1,0:T(8,128)(2,1)S(1)}, bf16[1,256,512]{2,1,0:T(8,128)(2,1)}, u32[]{:S(2)}) copy-start(bf16[1,256,512]{2,1,0:T(8,128)(2,1)} %get-tuple-element.21) | copy-start | bytes 786436
  136.5 45.1 %copy-start.8 = (f32[1,2048]{1,0:T(1,128)S(1)}, f32[1,2048]{1,0:T(1,128)}, u32[]{:S(2)}) copy-start(f32[1,2048]{1,0:T(1,128)} %get-tuple-element.28) | copy-start | bytes 24580
  136.6 45.1 %all-gather.36.cloned.1.call-start = ((), (), s32[]{:S(2)}) async-start(), calls=%async_computation.10 | async-start | bytes 1310720 | tf_op jit(solution)/shard_map/all_gather | solution.py:73
  137.1 74.3 %all-gather.38.cloned.1.call-start = ((), (), s32[]{:S(2)}) async-start(), calls=%async_computation.11 | async-start | bytes 1310720 | tf_op jit(solution)/shard_map/all_gather | solution.py:98
  138.1 119.2 %all-gather.34.cloned.1.call-start = ((), (), s32[]{:S(2)}) async-start(), calls=%async_computation.9 | async-start | bytes 2621440 | tf_op jit(solution)/shard_map/all_gather | solution.py:78
  153.8 60.0 %copy-start.24 = (f32[256]{0:T(256)}, f32[256]{0:T(256)S(1)}, u32[]{:S(2)}) copy-start(f32[256]{0:T(256)S(1)} %add_rsqrt_fusion.1) | copy-start | bytes 3076
  183.7 33.6 %collective-permute-start.2 = (bf16[8,32,256]{2,1,0:T(8,128)(2,1)S(1)}, bf16[8,32,256]{2,1,0:T(8,128)(2,1)S(1)}, u32[]{:S(2)}, u32[]{:S(2)}) collective-permute-start(bf16[8,32,256]{2,1,0:T(8,128)(2,1)S(1)} %bitcast.107), channel_id=1, source_target_pairs={{0,4},{4,8},{8,12},{1,5},{5,9},{9,13},{2,6},{6,10},{10,14},{3,7},{... | collective-permute-start | bytes 393224 | tf_op jit(solution)/shard_map/ppermute | solution.py:21
  187.1 30.3 %collective-permute-start.3 = (bf16[8,32,256]{2,1,0:T(8,128)(2,1)S(1)}, bf16[8,32,256]{2,1,0:T(8,128)(2,1)S(1)}, u32[]{:S(2)}, u32[]{:S(2)}) collective-permute-start(bf16[8,32,256]{2,1,0:T(8,128)(2,1)S(1)} %bitcast.108), channel_id=1, source_target_pairs={{4,0},{8,4},{12,8},{5,1},{9,5},{13,9},{6,2},{10,6},{14,10},{7,3},{... | collective-permute-start | bytes 393224 | tf_op jit(solution)/shard_map/ppermute | solution.py:22
  213.7 21.8 %all-to-all-start.1 = ((bf16[256,4,512]{2,0,1:T(8,128)(2,1)}), bf16[256,4,512]{2,0,1:T(8,128)(2,1)S(1)}, u32[]{:S(2)}, u32[]{:S(2)}) async-start(bf16[256,4,512]{2,0,1:T(8,128)(2,1)} %copy.24), calls=%async_computation.1 | async-start | bytes 2097152 | tf_op jit(solution)/shard_map/all_to_all | solution.py:99
  217.3 58.8 %all-gather.26.cloned.1.call-start = ((), (), s32[]{:S(2)}) async-start(), calls=%async_computation.5 | async-start | bytes 1310720 | tf_op jit(solution)/shard_map/all_gather | solution.py:64
  217.7 0.6 copy-start.12
  217.7 0.6 copy-start.15
  217.7 0.7 copy-start.18
  217.7 0.7 copy-start.21
  219.2 38.1 %copy-start.3 = (bf16[256,2048]{1,0:T(8,128)(2,1)S(1)}, bf16[256,2048]{1,0:T(8,128)(2,1)}, u32[]{:S(2)}) copy-start(bf16[256,2048]{1,0:T(8,128)(2,1)} %all-gather.24.cloned.1.call-done) | copy-start | bytes 3145732
  219.2 38.0 %copy-start.9 = (f32[1,2048]{1,0:T(1,128)S(1)}, f32[1,2048]{1,0:T(1,128)}, u32[]{:S(2)}) copy-start(f32[1,2048]{1,0:T(1,128)} %get-tuple-element.28) | copy-start | bytes 24580
  219.2 38.0 %copy-start.25 = (f32[256]{0:T(256)S(1)}, f32[256]{0:T(256)}, u32[]{:S(2)}) copy-start(f32[256]{0:T(256)} %copy-done.24) | copy-start | bytes 3076
  260.4 45.1 %copy-start.7 = (f32[1,2048]{1,0:T(1,128)S(1)}, f32[1,2048]{1,0:T(1,128)}, u32[]{:S(2)}) copy-start(f32[1,2048]{1,0:T(1,128)} %get-tuple-element.26) | copy-start | bytes 24580
  260.4 45.1 %all-gather.42.cloned.1.call-start = ((), (), s32[]{:S(2)}) async-start(), calls=%async_computation.13 | async-start | bytes 1310720 | tf_op jit(solution)/shard_map/all_gather | solution.py:73
  261.0 74.3 %all-gather.44.cloned.1.call-start = ((), (), s32[]{:S(2)}) async-start(), calls=%async_computation.14 | async-start | bytes 1310720 | tf_op jit(solution)/shard_map/all_gather | solution.py:98
  261.9 119.0 %all-gather.40.cloned.1.call-start = ((), (), s32[]{:S(2)}) async-start(), calls=%async_computation.12 | async-start | bytes 2621440 | tf_op jit(solution)/shard_map/all_gather | solution.py:78
  307.6 33.7 %collective-permute-start.4 = (bf16[8,32,256]{2,1,0:T(8,128)(2,1)S(1)}, bf16[8,32,256]{2,1,0:T(8,128)(2,1)S(1)}, u32[]{:S(2)}, u32[]{:S(2)}) collective-permute-start(bf16[8,32,256]{2,1,0:T(8,128)(2,1)S(1)} %bitcast.103), channel_id=1, source_target_pairs={{0,4},{4,8},{8,12},{1,5},{5,9},{9,13},{2,6},{6,10},{10,14},{3,7},{... | collective-permute-start | bytes 393224 | tf_op jit(solution)/shard_map/ppermute | solution.py:21
  310.9 30.4 %collective-permute-start.5 = (bf16[8,32,256]{2,1,0:T(8,128)(2,1)S(1)}, bf16[8,32,256]{2,1,0:T(8,128)(2,1)S(1)}, u32[]{:S(2)}, u32[]{:S(2)}) collective-permute-start(bf16[8,32,256]{2,1,0:T(8,128)(2,1)S(1)} %bitcast.104), channel_id=1, source_target_pairs={{4,0},{8,4},{12,8},{5,1},{9,5},{13,9},{6,2},{10,6},{14,10},{7,3},{... | collective-permute-start | bytes 393224 | tf_op jit(solution)/shard_map/ppermute | solution.py:22
  337.6 21.8 %all-to-all-start.2 = ((bf16[256,4,512]{2,0,1:T(8,128)(2,1)}), bf16[256,4,512]{2,0,1:T(8,128)(2,1)S(1)}, u32[]{:S(2)}, u32[]{:S(2)}) async-start(bf16[256,4,512]{2,0,1:T(8,128)(2,1)} %copy.28), calls=%async_computation.2 | async-start | bytes 2097152 | tf_op jit(solution)/shard_map/all_to_all | solution.py:99
  341.6 0.6 copy-start.13
  341.6 0.6 copy-start.16
  341.6 0.7 copy-start.19
  341.6 0.7 copy-start.22
  343.1 37.9 %copy-start.2 = (bf16[256,2048]{1,0:T(8,128)(2,1)S(1)}, bf16[256,2048]{1,0:T(8,128)(2,1)}, u32[]{:S(2)}) copy-start(bf16[256,2048]{1,0:T(8,128)(2,1)} %all-gather.26.cloned.1.call-done) | copy-start | bytes 3145732
Sparse Core Ops, SparseCore 0:
  8.9 19.4 all-gather.21
  29.9 27.9 all-gather.29
  59.5 28.1 all-gather.31
  89.1 44.1 all-gather.27
  136.7 15.4 all-gather.23
  153.7 27.9 all-gather.35
  183.2 28.1 all-gather.37
  213.0 44.1 all-gather.33
  260.6 15.4 all-gather.25
  277.5 27.9 all-gather.41
  307.1 28.1 all-gather.43
  336.7 44.2 all-gather.39
where the time goes:
time: 392 us; the launch traced here: 391 us
  waiting for transfers between devices  261 us (67%)
  blocking collectives  48.8 us (12%)
  starting transfers between devices  25.1 us (6%)
  matrix products  16.9 us (4%)
  local copies, waits for them, and re-layouts  15.8 us (4%)
  between operations  14.2 us (4%)
  other arithmetic  8.76 us (2%)
    all_gather x3, waiting for transfers between devices, on_device(): lax.all_gather(w_pool_in[layer_id], 'sp', axis=0, tiled=True)  83.9 us
    all_gather x3, waiting for transfers between devices, on_device(): back_rows = lax.all_gather(w_back[layer_id], 'sp', axis=1, tiled=True)  69.2 us
    all_gather x3, waiting for transfers between devices, on_device(): lax.all_gather(w_gate[layer_id], 'sp', axis=0, tiled=True)  63.4 us
    all_gather x3, blocking collectives, on_device(): full_pooled = lax.all_gather(pooled, 'tp', axis=1, tiled=True)  48.8 us
    all_gather x3, waiting for transfers between devices, on_device(): whole_rows = lax.all_gather(state, 'tp', axis=1, tiled=True)  41.8 us
    all_to_all x3, starting transfers between devices, on_device(): lax.all_to_all(back_rows, 'tp', split_axis=1, concat_axis=0, tiled=True)  10.7 us
    ppermute x3, starting transfers between devices, padded_2(): before = lax.ppermute(last, axis, up)  10.1 us
    dot_general x3, matrix products, on_device(): jnp.dot(normed, lax.all_gather(w_gate[layer_id], 'sp', axis=0, tiled=True...  9.41 us
  transfers between devices with their start and end apart: 21, of which 12 were waited for; matrix products, arithmetic and copies ran while one was open for 8% of the time, Pallas kernels for 0%

commit v1 on v0

--- a/solution.py
+++ b/solution.py
@@ -95,7 +95,14 @@
             (means - cells.astype(jnp.float32)).reshape(tok_rows, local_pool).astype(jnp.bfloat16)
         )
         full_pooled = lax.all_gather(pooled, "tp", axis=1, tiled=True)
-        back_rows = lax.all_gather(w_back[layer_id], "sp", axis=1, tiled=True)
+        ring = [w_back[layer_id]]
+        for hop in range(3):
+            ring.append(lax.ppermute(ring[-1], "sp", [(dev, (dev + 1) % 4) for dev in range(4)]))
+        back_rows = jnp.roll(
+            jnp.concatenate(ring[::-1], axis=1),
+            (lax.axis_index("sp") + 1) * ring[0].shape[1],
+            axis=1,
+        )
         back_cols = lax.all_to_all(back_rows, "tp", split_axis=1, concat_axis=0, tiled=True)
         partials = jnp.einsum(
             "tnb,nbd->ntd",

time: 392 us -> 315 us (0.80)
  waiting for transfers between devices: 261 us -> 166 us
  other arithmetic: 8.76 us -> 31.9 us
  local copies, waits for them, and re-layouts: 15.8 us -> 10.9 us
    all_gather x3 -> x0, waiting for transfers between devices: 69.2 us -> none  [on_device(): back_rows = lax.all_gather(w_back[layer_id], 'sp', axis=1, tiled=True)]
    ppermute x0 -> x9, waiting for transfers between devices: none -> 41.2 us  [on_device(): lax.ppermute(ring[-1], 'sp', [(dev, (dev + 1) % 4) for dev in range(4)])]
    all_gather x3, waiting for transfers between devices: 63.4 us -> 25.9 us  [on_device(): lax.all_gather(w_gate[layer_id], 'sp', axis=0, tiled=True)]
    all_gather x3, waiting for transfers between devices: 41.8 us -> 13.9 us  [on_device(): whole_rows = lax.all_gather(state, 'tp', axis=1, tiled=True)]
    concatenate x0 -> x2, other arithmetic: none -> 22 us  [on_device(): jnp.roll(jnp.concatenate(ring[::-1], axis=1), (lax.axis_index('sp') + 1)...]
    ppermute x0 -> x9, starting transfers between devices: none -> 4.99 us  [on_device(): lax.ppermute(ring[-1], 'sp', [(dev, (dev + 1) % 4) for dev in range(4)])]
    all_gather x3, waiting for transfers between devices: 83.9 us -> 78.9 us  [on_device(): lax.all_gather(w_pool_in[layer_id], 'sp', axis=0, tiled=True)]
  transfers between devices with their start and end apart: 21 -> 27, of which waited for: 12 -> 14; matrix products, arithmetic and copies ran while one was open for 8% -> 16% of each run, Pallas kernels for 0% -> 0%
where the time goes in v1:
time: 315 us; the launch traced here: 314 us
  waiting for transfers between devices  166 us (53%)
  blocking collectives  45.2 us (14%)
  other arithmetic  31.9 us (10%)
  starting transfers between devices  29 us (9%)
  matrix products  17.3 us (5%)
  between operations  13.8 us (4%)
  local copies, waits for them, and re-layouts  10.9 us (3%)
    all_gather x3, waiting for transfers between devices, on_device(): lax.all_gather(w_pool_in[layer_id], 'sp', axis=0, tiled=True)  78.9 us
    all_gather x3, blocking collectives, on_device(): full_pooled = lax.all_gather(pooled, 'tp', axis=1, tiled=True)  45.2 us
    ppermute x9, waiting for transfers between devices, on_device(): lax.ppermute(ring[-1], 'sp', [(dev, (dev + 1) % 4) for dev in range(4)])  41.2 us
    all_gather x3, waiting for transfers between devices, on_device(): lax.all_gather(w_gate[layer_id], 'sp', axis=0, tiled=True)  25.9 us
    concatenate x2, other arithmetic, on_device(): jnp.roll(jnp.concatenate(ring[::-1], axis=1), (lax.axis_index('sp') + 1)...  22 us
    all_gather x3, waiting for transfers between devices, on_device(): whole_rows = lax.all_gather(state, 'tp', axis=1, tiled=True)  13.9 us
    all_to_all x3, starting transfers between devices, on_device(): lax.all_to_all(back_rows, 'tp', split_axis=1, concat_axis=0, tiled=True)  10.5 us
    dot_general x3, matrix products, on_device(): jnp.dot(normed, lax.all_gather(w_gate[layer_id], 'sp', axis=0, tiled=True...  9.73 us
  transfers between devices with their start and end apart: 27, of which 14 were waited for; matrix products, arithmetic and copies ran while one was open for 16% of the time, Pallas kernels for 0%

profile of v1, /device:TPU:0, one launch (start us, length us, event | category | flops | bytes accessed | tf_op | source)
XLA Modules:
  0.0 314.0 jit_solution(10059739187569393528)
XLA Ops:
  7.3 2.0 fusion.189
  10.3 3.1 collective-permute-start.2
  13.4 1.2 fusion.187
  15.6 6.1 %collective-permute-done.2 = bf16[256,512]{0,1:T(8,128)(2,1)S(1)} collective-permute-done((bf16[256,512]{0,1:T(8,128)(2,1)S(1)}, bf16[256,512]{0,1:T(8,128)(2,1)S(1)}, u32[]{:S(2)}, u32[]{:S(2)}) %collective-permute-start.2) | collective-permute-done | bytes 262176 | tf_op jit(solution)/shard_map/ppermute | solution.py:100
  21.9 9.1 %collective-permute-done.3 = bf16[256,512]{0,1:T(8,128)(2,1)S(1)} collective-permute-done((bf16[256,512]{0,1:T(8,128)(2,1)S(1)}, bf16[256,512]{0,1:T(8,128)(2,1)S(1)}, u32[]{:S(2)}, u32[]{:S(2)}) %collective-permute-start.3) | collective-permute-done | bytes 262176 | tf_op jit(solution)/shard_map/ppermute | solution.py:100
  31.0 1.5 fusion
  32.5 25.4 %all-gather.24.cloned.1.call-done = bf16[1,2048,256]{2,1,0:T(8,128)(2,1)} async-done(((bf16[1,512,256]{2,1,0:T(8,128)(2,1)}), bf16[1,2048,256]{2,1,0:T(8,128)(2,1)}) %all-gather.24.cloned.1.call-update) | async-done | bytes 1048592 | tf_op jit(solution)/shard_map/all_gather | solution.py:73
  57.9 2.0 convolution_convert_fusion.5
  60.0 3.4 %collective-permute-start = (bf16[8,32,256]{2,1,0:T(8,128)(2,1)S(1)}, bf16[8,32,256]{2,1,0:T(8,128)(2,1)S(1)}, u32[]{:S(2)}, u32[]{:S(2)}) collective-permute-start(bf16[8,32,256]{2,1,0:T(8,128)(2,1)S(1)} %bitcast.112), channel_id=1, source_target_pairs={{0,4},{4,8},{8,12},{1,5},{5,9},{9,13},{2,6},{6,10},{10,14},{3,7},{... | collective-permute-start | bytes 393224 | tf_op jit(solution)/shard_map/ppermute | solution.py:21
  63.3 1.3 collective-permute-start.1
  64.6 9.6 %fusion.96 = bf16[256,2048]{0,1:T(8,128)(2,1)S(1)} fusion(s32[]{:T(128)S(6)} %select_n.83, bf16[256,512]{0,1:T(8,128)(2,1)S(1)} %collective-permute-done.4, bf16[256,512]{0,1:T(8,128)(2,1)S(1)} %collective-permute-done.3, bf16[256,512]{0,1:T(8,128)(2,1)S(1)} %collective-permute-done.2, bf16[256,512]{0,1:T(8,128)(2,1)S(1)} %bitcast.103), kind=kLoop, calls=%fused_computation.95 | loop fusion | flops 8388608 | bytes 2097156 | tf_op jit(solution)/shard_map/jit(_roll_dynamic)/concatenate | solution.py:101
  74.3 1.3 copy.20
  75.6 3.5 %all-to-all-start = ((bf16[256,4,512]{2,0,1:T(8,128)(2,1)}), bf16[256,4,512]{2,0,1:T(8,128)(2,1)S(1)}, u32[]{:S(2)}, u32[]{:S(2)}) async-start(bf16[256,4,512]{2,0,1:T(8,128)(2,1)} %copy.20), calls=%async_computation | async-start | bytes 2097152 | tf_op jit(solution)/shard_map/all_to_all | solution.py:106
  79.7 0.8 fusion.172
  80.6 16.6 %all_gather.39 = bf16[256,1024]{1,0:T(8,128)(2,1)S(1)} all-gather(bf16[256,256]{1,0:T(8,128)(2,1)S(1)} %bitcast.121), channel_id=1, replica_groups=mesh['grp'=2,'sp'=4,'tp'=4] {'tp'}, dimensions={1}, use_global_device_ids=true | all-gather | bytes 655360 | tf_op jit(solution)/shard_map/all_gather | solution.py:97
  97.9 6.7 %all-gather.22.cloned.1.call-done = bf16[1,2048,512]{2,1,0:T(8,128)(2,1)} async-done(((bf16[1,512,512]{2,1,0:T(8,128)(2,1)}), bf16[1,2048,512]{2,1,0:T(8,128)(2,1)}) %all-gather.22.cloned.1.call-update) | async-done | bytes 2097168 | tf_op jit(solution)/shard_map/all_gather | solution.py:78
  104.6 3.1 fusion.75
  108.9 1.6 collective-permute-start.7
  110.6 9.0 %collective-permute-done.12 = bf16[256,512]{0,1:T(8,128)(2,1)S(1)} collective-permute-done((bf16[256,512]{0,1:T(8,128)(2,1)S(1)}, bf16[256,512]{0,1:T(8,128)(2,1)S(1)}, u32[]{:S(2)}, u32[]{:S(2)}) %collective-permute-start.12) | collective-permute-done | bytes 262176 | tf_op jit(solution)/shard_map/ppermute | solution.py:100
  119.6 5.6 %collective-permute-done.7 = bf16[256,512]{0,1:T(8,128)(2,1)S(1)} collective-permute-done((bf16[256,512]{0,1:T(8,128)(2,1)S(1)}, bf16[256,512]{0,1:T(8,128)(2,1)S(1)}, u32[]{:S(2)}, u32[]{:S(2)}) %collective-permute-start.7) | collective-permute-done | bytes 262176 | tf_op jit(solution)/shard_map/ppermute | solution.py:100
  125.2 5.6 %collective-permute-done.13 = bf16[256,512]{0,1:T(8,128)(2,1)S(1)} collective-permute-done((bf16[256,512]{0,1:T(8,128)(2,1)S(1)}, bf16[256,512]{0,1:T(8,128)(2,1)S(1)}, u32[]{:S(2)}, u32[]{:S(2)}) %collective-permute-start.13) | collective-permute-done | bytes 262176 | tf_op jit(solution)/shard_map/ppermute | solution.py:100
  130.8 5.7 %collective-permute-done.8 = bf16[256,512]{0,1:T(8,128)(2,1)S(1)} collective-permute-done((bf16[256,512]{0,1:T(8,128)(2,1)S(1)}, bf16[256,512]{0,1:T(8,128)(2,1)S(1)}, u32[]{:S(2)}, u32[]{:S(2)}) %collective-permute-start.8) | collective-permute-done | bytes 262176 | tf_op jit(solution)/shard_map/ppermute | solution.py:100
  136.6 1.6 fusion.3
  138.2 25.4 %all-gather.28.cloned.1.call-done = bf16[1,2048,256]{2,1,0:T(8,128)(2,1)} async-done(((bf16[1,512,256]{2,1,0:T(8,128)(2,1)}), bf16[1,2048,256]{2,1,0:T(8,128)(2,1)}) %all-gather.28.cloned.1.call-update) | async-done | bytes 1048592 | tf_op jit(solution)/shard_map/all_gather | solution.py:73
  163.6 2.0 convolution_convert_fusion.4
  165.7 2.6 collective-permute-start.5
  168.2 1.3 collective-permute-start.6
  170.3 12.4 %fusion.82 = (bf16[256,2048]{0,1:T(8,128)(2,1)S(1)}, bf16[256,2048]{0,1:T(8,128)(2,1)S(1)}) fusion(s32[]{:T(128)S(6)} %select_n.83, bf16[256,512]{0,1:T(8,128)(2,1)} %copy-done.6, bf16[256,512]{0,1:T(8,128)(2,1)S(1)} %collective-permute-done.13, bf16[256,512]{0,1:T(8,128)(2,1)S(1)} %collective-permute-done.12, bf16[256,512]{0,1:T(8,128)(2,1)S(1)} %bitcast.105, ...), kind=kLoop, calls=%fused_computation.81 | loop fusion | flops 16777216 | bytes 4194308 | tf_op jit(solution)/shard_map/jit(_roll_dynamic)/concatenate | solution.py:101
  182.7 1.3 copy.24
  184.0 3.5 %all-to-all-start.1 = ((bf16[256,4,512]{2,0,1:T(8,128)(2,1)}), bf16[256,4,512]{2,0,1:T(8,128)(2,1)S(1)}, u32[]{:S(2)}, u32[]{:S(2)}) async-start(bf16[256,4,512]{2,0,1:T(8,128)(2,1)} %copy.24), calls=%async_computation.1 | async-start | bytes 2097152 | tf_op jit(solution)/shard_map/all_to_all | solution.py:106
  187.6 1.1 fusion.113
  189.6 0.8 fusion.173
  190.5 15.1 %all_gather.43 = bf16[256,1024]{1,0:T(8,128)(2,1)S(1)} all-gather(bf16[256,256]{1,0:T(8,128)(2,1)S(1)} %bitcast.122), channel_id=1, replica_groups=mesh['grp'=2,'sp'=4,'tp'=4] {'tp'}, dimensions={1}, use_global_device_ids=true | all-gather | bytes 655360 | tf_op jit(solution)/shard_map/all_gather | solution.py:97
  206.3 2.9 all-gather.26.cloned.1.call-done
  209.2 3.5 %fusion.72 = bf16[256,512]{1,0:T(8,128)(2,1)} fusion(f32[256,512]{1,0:T(8,128)S(1)} %convert_reduce_fusion.1, bf16[1,2048,512]{2,1,0:T(8,128)(2,1)} %all-gather.26.cloned.1.call-done, bf16[256,512]{1,0:T(8,128)(2,1)S(1)} %copy-done.7, bf16[256,2048]{1,0:T(8,128)(2,1)} %all-gather.18.cloned.1.call-done, f32[2048]{0:T(1024)S(1)} %bitcast.126, ...), kind=kOutput, calls=%fused_computation.72 | convolution fusion | flops 539885568 | bytes 4203520 | tf_op jit(solution)/shard_map/dot_general | solution.py:76
  214.2 13.9 %all-gather.20.cloned.1.call-done = bf16[256,2048]{1,0:T(8,128)(2,1)} async-done(((bf16[256,512]{1,0:T(8,128)(2,1)}), bf16[256,2048]{1,0:T(8,128)(2,1)}) %all-gather.20.cloned.1.call-update) | async-done | bytes 1048592 | tf_op jit(solution)/shard_map/all_gather | solution.py:64
  228.1 1.5 fusion.6
  229.6 28.1 %all-gather.32.cloned.1.call-done = bf16[1,2048,256]{2,1,0:T(8,128)(2,1)} async-done(((bf16[1,512,256]{2,1,0:T(8,128)(2,1)}), bf16[1,2048,256]{2,1,0:T(8,128)(2,1)}) %all-gather.32.cloned.1.call-update) | async-done | bytes 1048592 | tf_op jit(solution)/shard_map/all_gather | solution.py:73
  257.7 2.0 convolution_convert_fusion.3
  259.7 3.4 %collective-permute-start.10 = (bf16[8,32,256]{2,1,0:T(8,128)(2,1)S(1)}, bf16[8,32,256]{2,1,0:T(8,128)(2,1)S(1)}, u32[]{:S(2)}, u32[]{:S(2)}) collective-permute-start(bf16[8,32,256]{2,1,0:T(8,128)(2,1)S(1)} %bitcast.116), channel_id=1, source_target_pairs={{0,4},{4,8},{8,12},{1,5},{5,9},{9,13},{2,6},{6,10},{10,14},{3,7},{... | collective-permute-start | bytes 393224 | tf_op jit(solution)/shard_map/ppermute | solution.py:21
  263.1 1.3 collective-permute-start.11
  264.4 1.3 copy.28
  265.7 3.5 %all-to-all-start.2 = ((bf16[256,4,512]{2,0,1:T(8,128)(2,1)}), bf16[256,4,512]{2,0,1:T(8,128)(2,1)S(1)}, u32[]{:S(2)}, u32[]{:S(2)}) async-start(bf16[256,4,512]{2,0,1:T(8,128)(2,1)} %copy.28), calls=%async_computation.2 | async-start | bytes 2097152 | tf_op jit(solution)/shard_map/all_to_all | solution.py:106
  269.2 3.3 %collective-permute-done.11 = bf16[8,32,256]{2,1,0:T(8,128)(2,1)S(1)} collective-permute-done((bf16[8,32,256]{2,1,0:T(8,128)(2,1)S(1)}, bf16[8,32,256]{2,1,0:T(8,128)(2,1)S(1)}, u32[]{:S(2)}, u32[]{:S(2)}) %collective-permute-start.11) | collective-permute-done | bytes 131104 | tf_op jit(solution)/shard_map/ppermute | solution.py:22
  273.0 0.8 fusion.174
  273.9 13.4 %all_gather.47 = bf16[256,1024]{1,0:T(8,128)(2,1)S(1)} all-gather(bf16[256,256]{1,0:T(8,128)(2,1)S(1)} %bitcast.120), channel_id=1, replica_groups=mesh['grp'=2,'sp'=4,'tp'=4] {'tp'}, dimensions={1}, use_global_device_ids=true | all-gather | bytes 655360 | tf_op jit(solution)/shard_map/all_gather | solution.py:97
  288.0 16.3 %all-gather.30.cloned.1.call-done = bf16[1,2048,512]{2,1,0:T(8,128)(2,1)} async-done(((bf16[1,512,512]{2,1,0:T(8,128)(2,1)}), bf16[1,2048,512]{2,1,0:T(8,128)(2,1)}) %all-gather.30.cloned.1.call-update) | async-done | bytes 2097168 | tf_op jit(solution)/shard_map/all_gather | solution.py:78
  304.3 3.1 fusion.69
  (116 shorter events, 10.0 us)
Async XLA Ops:
  6.5 2.9 copy-start.4
  6.5 6.9 %copy-start = (bf16[3,512,512]{2,1,0:T(8,128)(2,1)S(1)}, bf16[3,512,512]{2,1,0:T(8,128)(2,1)}, u32[]{:S(2)}) copy-start(bf16[3,512,512]{2,1,0:T(8,128)(2,1)} %param.10) | copy-start | bytes 4718596
  6.5 24.5 %all-gather.16.cloned.1.call-start = ((), (), s32[]{:S(2)}) async-start(), calls=%async_computation.3 | async-start | bytes 1310720 | tf_op jit(solution)/shard_map/all_gather | solution.py:64
  7.3 50.7 %all-gather.24.cloned.1.call-start = ((), (), s32[]{:S(2)}) async-start(), calls=%async_computation.7 | async-start | bytes 1310720 | tf_op jit(solution)/shard_map/all_gather | solution.py:73
  9.3 95.2 %all-gather.22.cloned.1.call-start = ((), (), s32[]{:S(2)}) async-start(), calls=%async_computation.6 | async-start | bytes 2621440 | tf_op jit(solution)/shard_map/all_gather | solution.py:78
  10.2 4.6 %copy-start.9 = (f32[3,2048]{1,0:T(4,128)S(1)}, f32[3,2048]{1,0:T(4,128)}, u32[]{:S(2)}) copy-start(f32[3,2048]{1,0:T(4,128)} %param.8) | copy-start | bytes 73732
  10.3 11.4 %collective-permute-start.2 = (bf16[256,512]{0,1:T(8,128)(2,1)S(1)}, bf16[256,512]{0,1:T(8,128)(2,1)S(1)}, u32[]{:S(2)}, u32[]{:S(2)}) collective-permute-start(bf16[256,512]{0,1:T(8,128)(2,1)S(1)} %bitcast.102), channel_id=1, source_target_pairs={{0,4},{4,8},{8,12},{12,0},{1,5},{5,9},{9,13},{13,1},{2,6},{6,10},{... | collective-permute-start | bytes 786440 | tf_op jit(solution)/shard_map/ppermute | solution.py:100
  15.5 64.2 %copy-start.13 = (pred[256]{0:T(512)(128)(4,1)}, pred[256]{0:T(512)(128)(4,1)S(1)}, u32[]{:S(2)}) copy-start(pred[256]{0:T(512)(128)(4,1)S(1)} %get-tuple-element.38) | copy-start | bytes 772
  15.5 64.2 %copy-start.15 = (pred[256]{0:T(512)(128)(4,1)}, pred[256]{0:T(512)(128)(4,1)S(1)}, u32[]{:S(2)}) copy-start(pred[256]{0:T(512)(128)(4,1)S(1)} %get-tuple-element.39) | copy-start | bytes 772
  21.7 9.3 %collective-permute-start.3 = (bf16[256,512]{0,1:T(8,128)(2,1)S(1)}, bf16[256,512]{0,1:T(8,128)(2,1)S(1)}, u32[]{:S(2)}, u32[]{:S(2)}) collective-permute-start(bf16[256,512]{0,1:T(8,128)(2,1)S(1)} %collective-permute-done.2), channel_id=1, source_target_pairs={{0,4},{4,8},{8,12},{12,0},{1,5},{5,9},{9,13},{13,1},{2,6},{6,10},{... | collective-permute-start | bytes 786440 | tf_op jit(solution)/shard_map/ppermute | solution.py:100
  21.7 57.9 %copy-start.17 = (pred[256]{0:T(512)(128)(4,1)}, pred[256]{0:T(512)(128)(4,1)S(1)}, u32[]{:S(2)}) copy-start(pred[256]{0:T(512)(128)(4,1)S(1)} %get-tuple-element.40) | copy-start | bytes 772
  21.8 57.9 %copy-start.19 = (pred[256]{0:T(512)(128)(4,1)}, pred[256]{0:T(512)(128)(4,1)S(1)}, u32[]{:S(2)}) copy-start(pred[256]{0:T(512)(128)(4,1)S(1)} %get-tuple-element.41) | copy-start | bytes 772
  31.0 33.6 %collective-permute-start.4 = (bf16[256,512]{0,1:T(8,128)(2,1)S(1)}, bf16[256,512]{0,1:T(8,128)(2,1)S(1)}, u32[]{:S(2)}, u32[]{:S(2)}) collective-permute-start(bf16[256,512]{0,1:T(8,128)(2,1)S(1)} %collective-permute-done.3), channel_id=1, source_target_pairs={{0,4},{4,8},{8,12},{12,0},{1,5},{5,9},{9,13},{13,1},{2,6},{6,10},{... | collective-permute-start | bytes 786440 | tf_op jit(solution)/shard_map/ppermute | solution.py:100
  60.0 19.2 %collective-permute-start = (bf16[8,32,256]{2,1,0:T(8,128)(2,1)S(1)}, bf16[8,32,256]{2,1,0:T(8,128)(2,1)S(1)}, u32[]{:S(2)}, u32[]{:S(2)}) collective-permute-start(bf16[8,32,256]{2,1,0:T(8,128)(2,1)S(1)} %bitcast.112), channel_id=1, source_target_pairs={{0,4},{4,8},{8,12},{1,5},{5,9},{9,13},{2,6},{6,10},{10,14},{3,7},{... | collective-permute-start | bytes 393224 | tf_op jit(solution)/shard_map/ppermute | solution.py:21
  63.3 15.9 %collective-permute-start.1 = (bf16[8,32,256]{2,1,0:T(8,128)(2,1)S(1)}, bf16[8,32,256]{2,1,0:T(8,128)(2,1)S(1)}, u32[]{:S(2)}, u32[]{:S(2)}) collective-permute-start(bf16[8,32,256]{2,1,0:T(8,128)(2,1)S(1)} %bitcast.113), channel_id=1, source_target_pairs={{4,0},{8,4},{12,8},{5,1},{9,5},{13,9},{6,2},{10,6},{14,10},{7,3},{... | collective-permute-start | bytes 393224 | tf_op jit(solution)/shard_map/ppermute | solution.py:22
  75.6 21.8 %all-to-all-start = ((bf16[256,4,512]{2,0,1:T(8,128)(2,1)}), bf16[256,4,512]{2,0,1:T(8,128)(2,1)S(1)}, u32[]{:S(2)}, u32[]{:S(2)}) async-start(bf16[256,4,512]{2,0,1:T(8,128)(2,1)} %copy.20), calls=%async_computation | async-start | bytes 2097152 | tf_op jit(solution)/shard_map/all_to_all | solution.py:106
  79.1 57.4 %all-gather.18.cloned.1.call-start = ((), (), s32[]{:S(2)}) async-start(), calls=%async_computation.4 | async-start | bytes 1310720 | tf_op jit(solution)/shard_map/all_gather | solution.py:64
  80.5 24.1 %copy-start.1 = (bf16[256,2048]{1,0:T(8,128)(2,1)S(1)}, bf16[256,2048]{1,0:T(8,128)(2,1)}, u32[]{:S(2)}) copy-start(bf16[256,2048]{1,0:T(8,128)(2,1)} %all-gather.16.cloned.1.call-done) | copy-start | bytes 3145732
  97.9 10.5 %copy-start.3 = (bf16[1,256,512]{2,1,0:T(8,128)(2,1)S(1)}, bf16[1,256,512]{2,1,0:T(8,128)(2,1)}, u32[]{:S(2)}) copy-start(bf16[1,256,512]{2,1,0:T(8,128)(2,1)} %get-tuple-element.21) | copy-start | bytes 786436
  107.7 55.9 %copy-start.11 = (f32[1,2048]{1,0:T(1,128)S(1)}, f32[1,2048]{1,0:T(1,128)}, u32[]{:S(2)}) copy-start(f32[1,2048]{1,0:T(1,128)} %get-tuple-element.29) | copy-start | bytes 24580
  107.8 55.9 %all-gather.28.cloned.1.call-start = ((), (), s32[]{:S(2)}) async-start(), calls=%async_computation.9 | async-start | bytes 1310720 | tf_op jit(solution)/shard_map/all_gather | solution.py:73
  108.3 100.9 %all-gather.26.cloned.1.call-start = ((), (), s32[]{:S(2)}) async-start(), calls=%async_computation.8 | async-start | bytes 2621440 | tf_op jit(solution)/shard_map/all_gather | solution.py:78
  108.5 11.0 %collective-permute-start.12 = (bf16[256,512]{0,1:T(8,128)(2,1)S(1)}, bf16[256,512]{0,1:T(8,128)(2,1)S(1)}, u32[]{:S(2)}, u32[]{:S(2)}) collective-permute-start(bf16[256,512]{0,1:T(8,128)(2,1)S(1)} %bitcast.104), channel_id=1, source_target_pairs={{0,4},{4,8},{8,12},{12,0},{1,5},{5,9},{9,13},{13,1},{2,6},{6,10},{... | collective-permute-start | bytes 786440 | tf_op jit(solution)/shard_map/ppermute | solution.py:100
  108.9 16.3 %collective-permute-start.7 = (bf16[256,512]{0,1:T(8,128)(2,1)S(1)}, bf16[256,512]{0,1:T(8,128)(2,1)S(1)}, u32[]{:S(2)}, u32[]{:S(2)}) collective-permute-start(bf16[256,512]{0,1:T(8,128)(2,1)S(1)} %bitcast.106), channel_id=1, source_target_pairs={{0,4},{4,8},{8,12},{12,0},{1,5},{5,9},{9,13},{13,1},{2,6},{6,10},{... | collective-permute-start | bytes 786440 | tf_op jit(solution)/shard_map/ppermute | solution.py:100
  119.6 11.2 %collective-permute-start.13 = (bf16[256,512]{0,1:T(8,128)(2,1)S(1)}, bf16[256,512]{0,1:T(8,128)(2,1)S(1)}, u32[]{:S(2)}, u32[]{:S(2)}) collective-permute-start(bf16[256,512]{0,1:T(8,128)(2,1)S(1)} %collective-permute-done.12), channel_id=1, source_target_pairs={{0,4},{4,8},{8,12},{12,0},{1,5},{5,9},{9,13},{13,1},{2,6},{6,10},{... | collective-permute-start | bytes 786440 | tf_op jit(solution)/shard_map/ppermute | solution.py:100
  125.2 11.4 %collective-permute-start.8 = (bf16[256,512]{0,1:T(8,128)(2,1)S(1)}, bf16[256,512]{0,1:T(8,128)(2,1)S(1)}, u32[]{:S(2)}, u32[]{:S(2)}) collective-permute-start(bf16[256,512]{0,1:T(8,128)(2,1)S(1)} %collective-permute-done.7), channel_id=1, source_target_pairs={{0,4},{4,8},{8,12},{12,0},{1,5},{5,9},{9,13},{13,1},{2,6},{6,10},{... | collective-permute-start | bytes 786440 | tf_op jit(solution)/shard_map/ppermute | solution.py:100
  130.8 38.7 %collective-permute-start.14 = (bf16[256,512]{0,1:T(8,128)(2,1)S(1)}, bf16[256,512]{0,1:T(8,128)(2,1)S(1)}, u32[]{:S(2)}, u32[]{:S(2)}) collective-permute-start(bf16[256,512]{0,1:T(8,128)(2,1)S(1)} %collective-permute-done.13), channel_id=1, source_target_pairs={{0,4},{4,8},{8,12},{12,0},{1,5},{5,9},{9,13},{13,1},{2,6},{6,10},{... | collective-permute-start | bytes 786440 | tf_op jit(solution)/shard_map/ppermute | solution.py:100
  136.6 33.0 %copy-start.5 = (bf16[256,512]{0,1:T(8,128)(2,1)}, bf16[256,512]{0,1:T(8,128)(2,1)S(1)}, u32[]{:S(2)}) copy-start(bf16[256,512]{0,1:T(8,128)(2,1)S(1)} %collective-permute-done.8) | copy-start | bytes 786436
  136.6 33.7 %collective-permute-start.9 = (bf16[256,512]{0,1:T(8,128)(2,1)S(1)}, bf16[256,512]{0,1:T(8,128)(2,1)}, u32[]{:S(2)}, u32[]{:S(2)}) collective-permute-start(bf16[256,512]{0,1:T(8,128)(2,1)S(1)} %collective-permute-done.8), channel_id=1, source_target_pairs={{0,4},{4,8},{8,12},{12,0},{1,5},{5,9},{9,13},{13,1},{2,6},{6,10},{... | collective-permute-start | bytes 786440 | tf_op jit(solution)/shard_map/ppermute | solution.py:100
  138.2 31.4 %copy-start.21 = (f32[256]{0:T(256)}, f32[256]{0:T(256)S(1)}, u32[]{:S(2)}) copy-start(f32[256]{0:T(256)S(1)} %add_rsqrt_fusion.1) | copy-start | bytes 3076
  165.7 21.9 %collective-permute-start.5 = (bf16[8,32,256]{2,1,0:T(8,128)(2,1)S(1)}, bf16[8,32,256]{2,1,0:T(8,128)(2,1)}, u32[]{:S(2)}, u32[]{:S(2)}) collective-permute-start(bf16[8,32,256]{2,1,0:T(8,128)(2,1)S(1)} %bitcast.108), channel_id=1, source_target_pairs={{0,4},{4,8},{8,12},{1,5},{5,9},{9,13},{2,6},{6,10},{10,14},{3,7},{... | collective-permute-start | bytes 393224 | tf_op jit(solution)/shard_map/ppermute | solution.py:21
  168.2 19.4 %collective-permute-start.6 = (bf16[8,32,256]{2,1,0:T(8,128)(2,1)S(1)}, bf16[8,32,256]{2,1,0:T(8,128)(2,1)}, u32[]{:S(2)}, u32[]{:S(2)}) collective-permute-start(bf16[8,32,256]{2,1,0:T(8,128)(2,1)S(1)} %bitcast.109), channel_id=1, source_target_pairs={{4,0},{8,4},{12,8},{5,1},{9,5},{13,9},{6,2},{10,6},{14,10},{7,3},{... | collective-permute-start | bytes 393224 | tf_op jit(solution)/shard_map/ppermute | solution.py:22
  169.6 0.7 copy-start.6
  184.0 21.8 %all-to-all-start.1 = ((bf16[256,4,512]{2,0,1:T(8,128)(2,1)}), bf16[256,4,512]{2,0,1:T(8,128)(2,1)S(1)}, u32[]{:S(2)}, u32[]{:S(2)}) async-start(bf16[256,4,512]{2,0,1:T(8,128)(2,1)} %copy.24), calls=%async_computation.1 | async-start | bytes 2097152 | tf_op jit(solution)/shard_map/all_to_all | solution.py:106
  187.6 40.5 %all-gather.20.cloned.1.call-start = ((), (), s32[]{:S(2)}) async-start(), calls=%async_computation.5 | async-start | bytes 1310720 | tf_op jit(solution)/shard_map/all_gather | solution.py:64
  189.0 0.7 copy-start.14
  189.0 0.7 copy-start.16
  190.5 18.7 %copy-start.7 = (bf16[256,512]{1,0:T(8,128)(2,1)S(1)}, bf16[256,512]{1,0:T(8,128)(2,1)}, u32[]{:S(2)}) copy-start(bf16[256,512]{1,0:T(8,128)(2,1)} %fusion.75) | copy-start | bytes 786436
  190.5 18.7 %copy-start.12 = (f32[1,2048]{1,0:T(1,128)S(1)}, f32[1,2048]{1,0:T(1,128)}, u32[]{:S(2)}) copy-start(f32[1,2048]{1,0:T(1,128)} %get-tuple-element.29) | copy-start | bytes 24580
  190.5 18.7 %copy-start.22 = (f32[256]{0:T(256)S(1)}, f32[256]{0:T(256)}, u32[]{:S(2)}) copy-start(f32[256]{0:T(256)} %copy-done.21) | copy-start | bytes 3076
  212.7 45.0 %copy-start.10 = (f32[1,2048]{1,0:T(1,128)S(1)}, f32[1,2048]{1,0:T(1,128)}, u32[]{:S(2)}) copy-start(f32[1,2048]{1,0:T(1,128)} %get-tuple-element.27) | copy-start | bytes 24580
  212.7 45.0 %all-gather.32.cloned.1.call-start = ((), (), s32[]{:S(2)}) async-start(), calls=%async_computation.11 | async-start | bytes 1310720 | tf_op jit(solution)/shard_map/all_gather | solution.py:73
  213.5 90.9 %all-gather.30.cloned.1.call-start = ((), (), s32[]{:S(2)}) async-start(), calls=%async_computation.10 | async-start | bytes 2621440 | tf_op jit(solution)/shard_map/all_gather | solution.py:78
  259.7 9.5 %collective-permute-start.10 = (bf16[8,32,256]{2,1,0:T(8,128)(2,1)S(1)}, bf16[8,32,256]{2,1,0:T(8,128)(2,1)S(1)}, u32[]{:S(2)}, u32[]{:S(2)}) collective-permute-start(bf16[8,32,256]{2,1,0:T(8,128)(2,1)S(1)} %bitcast.116), channel_id=1, source_target_pairs={{0,4},{4,8},{8,12},{1,5},{5,9},{9,13},{2,6},{6,10},{10,14},{3,7},{... | collective-permute-start | bytes 393224 | tf_op jit(solution)/shard_map/ppermute | solution.py:21
  263.1 9.5 %collective-permute-start.11 = (bf16[8,32,256]{2,1,0:T(8,128)(2,1)S(1)}, bf16[8,32,256]{2,1,0:T(8,128)(2,1)S(1)}, u32[]{:S(2)}, u32[]{:S(2)}) collective-permute-start(bf16[8,32,256]{2,1,0:T(8,128)(2,1)S(1)} %bitcast.117), channel_id=1, source_target_pairs={{4,0},{8,4},{12,8},{5,1},{9,5},{13,9},{6,2},{10,6},{14,10},{7,3},{... | collective-permute-start | bytes 393224 | tf_op jit(solution)/shard_map/ppermute | solution.py:22
  265.7 21.8 %all-to-all-start.2 = ((bf16[256,4,512]{2,0,1:T(8,128)(2,1)}), bf16[256,4,512]{2,0,1:T(8,128)(2,1)S(1)}, u32[]{:S(2)}, u32[]{:S(2)}) async-start(bf16[256,4,512]{2,0,1:T(8,128)(2,1)} %copy.28), calls=%async_computation.2 | async-start | bytes 2097152 | tf_op jit(solution)/shard_map/all_to_all | solution.py:106
  273.8 30.5 %copy-start.2 = (bf16[256,2048]{1,0:T(8,128)(2,1)S(1)}, bf16[256,2048]{1,0:T(8,128)(2,1)}, u32[]{:S(2)}) copy-start(bf16[256,2048]{1,0:T(8,128)(2,1)} %all-gather.20.cloned.1.call-done) | copy-start | bytes 3145732
  273.9 30.5 %copy-start.8 = (bf16[256,512]{1,0:T(8,128)(2,1)S(1)}, bf16[256,512]{1,0:T(8,128)(2,1)}, u32[]{:S(2)}) copy-start(bf16[256,512]{1,0:T(8,128)(2,1)} %fusion.72) | copy-start | bytes 786436
  (2 other events, 1.3 us)
Sparse Core Ops, SparseCore 0:
  8.9 19.4 all-gather.15
  29.9 27.9 all-gather.23
  59.5 45.0 all-gather.21
  107.9 15.4 all-gather.17
  124.8 38.7 all-gather.27
  165.0 44.1 all-gather.25
  212.8 15.2 all-gather.19
  229.7 27.9 all-gather.31
  259.3 45.0 all-gather.29
